TPU v7x, 32 devices: a whole 2x2x4 slice. The times are simulated.
32 devices in a mesh: ep: 8 (over z, x), tp: 4 (over y, core).
Axes of the slice: x: 2, y: 2, z: 4, core: 2. Of those that a mesh axis runs over, the one named last changes fastest.
Arguments:
- conv_input: bfloat16 [8192, 2048], P('ep', 'tp'), may hold values from -6 to 6
- conv_kernel: bfloat16 [31, 2048], P(None, 'tp'), may hold values from -2 to 2
- norm_gain: float32 [2048], P('tp'), may hold values from 0.1 to 1.9
- norm_shift: float32 [2048], P('tp'), may hold values from -3 to 3
- conv_proj: bfloat16 [2048, 2048], P('tp'), may hold values from -0.125 to 0.125
- moe_input: bfloat16 [2048, 2048], P(('ep', 'tp')), may hold values from -6 to 6
- moe_gain: float32 [2048], replicated, may hold values from 0.1 to 1.9
- routes: int32 [2048, 2], P('ep'), may hold values from 0 to 7, all different within a row; in each aligned block of 256 rows (0 to 255, 256 to 511, ...) at most 128 rows name the same one
- route_weights: float32 [2048, 2], P('ep'), may hold values from 0.2 to 1
- gate_proj: bfloat16 [8, 2048, 2048], P('ep', None, 'tp'), may hold values from -0.125 to 0.125
- up_proj: bfloat16 [8, 2048, 2048], P('ep', None, 'tp'), may hold values from -0.125 to 0.125
- down_proj: bfloat16 [8, 2048, 2048], P('ep', 'tp'), may hold values from -0.125 to 0.125
Outputs:
- conv_out: bfloat16 [8192, 2048], P(('ep', 'tp'))
- moe_out: bfloat16 [2048, 2048], P(('ep', 'tp'))
Inputs may be any that keep to these rules, and one draw needn't show every extreme that they name: `routes`: each row names 2 different experts. In each aligned block of 256 rows no expert is named by more than 128 rows, and in some blocks an expert is named by exactly 128 rows.
All inputs are finite; a program needn't handle non-finite values.
Results may differ from a plain program's by a relative error of at most 0.012.
Values may be sent and summed in bfloat16 or wider, within the bound.
A program may use at most 128 MiB of HBM per device.

v0:
```python
import jax
import jax.numpy as jnp
from jax import lax
from jax.sharding import PartitionSpec as P


def shifted(value, axis, steps):
    count = lax.axis_size(axis)
    leading, last = (max(0, -steps), min(count, count - steps))
    return lax.ppermute(value, axis, [(source, source + steps) for source in range(leading, last)])


def local(
    conv_input,
    conv_kernel,
    norm_gain,
    norm_shift,
    conv_proj,
    moe_input,
    moe_gain,
    routes,
    route_weights,
    gate_proj,
    up_proj,
    down_proj,
):
    tp_count = lax.axis_size("tp")
    ep_count = lax.axis_size("ep")
    local_rows, local_width = conv_input.shape
    reach = conv_kernel.shape[0] - 1
    history = shifted(conv_input[local_rows - reach :], "ep", 1)
    padded = jnp.concatenate([history, conv_input], axis=0)
    taps = conv_kernel.astype(jnp.float32)
    mixed = jnp.zeros((local_rows, local_width), jnp.float32)
    for offset in range(reach + 1):
        mixed = mixed + padded[offset : offset + local_rows].astype(jnp.float32) * taps[offset]
    full_width = local_width * tp_count
    sums, squares = lax.psum((jnp.sum(mixed, axis=1), jnp.sum(mixed * mixed, axis=1)), "tp")
    center = sums / full_width
    spread = jnp.maximum(squares / full_width - center * center, 0.0)
    scaled = (mixed - center[:, None]) * lax.rsqrt(spread[:, None] + 1e-05) * norm_gain + norm_shift
    activated = jax.nn.silu(scaled).astype(jnp.bfloat16)
    conv_out = lax.psum_scatter(
        jnp.dot(activated, conv_proj, preferred_element_type=jnp.float32).astype(jnp.bfloat16),
        "tp",
        scatter_dimension=0,
        tiled=True,
    )
    moe_float = moe_input.astype(jnp.float32)
    normed = (
        moe_float
        * lax.rsqrt(jnp.mean(moe_float * moe_float, axis=1, keepdims=True) + 1e-06)
        * moe_gain
    ).astype(jnp.bfloat16)
    group = lax.all_gather(normed, "tp", axis=0, tiled=True)
    group_rows, top_count = routes.shape
    model_width = group.shape[1]
    capacity = 2 * top_count * group_rows // ep_count
    expert_ids = routes.reshape(-1)
    onehot = (expert_ids[:, None] == jnp.arange(ep_count, dtype=jnp.int32)[None, :]).astype(
        jnp.int32
    )
    ranks = jnp.sum((jnp.cumsum(onehot, axis=0) - onehot) * onehot, axis=1)
    targets = ranks * ep_count + expert_ids
    owners = jnp.arange(group_rows * top_count, dtype=jnp.int32) // top_count
    table = jnp.full((capacity * ep_count,), group_rows, jnp.int32).at[targets].set(owners)
    extended = jnp.concatenate([group, jnp.zeros((1, model_width), jnp.bfloat16)], axis=0)
    outgoing = extended[table].reshape(capacity, ep_count, model_width)
    share = capacity // tp_count
    own_slots = lax.dynamic_slice_in_dim(outgoing, lax.axis_index("tp") * share, share, 0)
    landed = lax.all_to_all(own_slots, "ep", split_axis=1, concat_axis=1, tiled=True)
    arrived = lax.all_gather(landed, "tp", axis=0, tiled=True)
    incoming = arrived.reshape(capacity * ep_count, model_width)
    gated = jax.nn.silu(jnp.dot(incoming, gate_proj[0], preferred_element_type=jnp.float32))
    hidden = (gated * jnp.dot(incoming, up_proj[0], preferred_element_type=jnp.float32)).astype(
        jnp.bfloat16
    )
    weights_flat = route_weights.reshape(-1)
    pieces = jnp.dot(hidden, down_proj[0], preferred_element_type=jnp.float32).astype(jnp.bfloat16)
    returned = lax.all_to_all(
        pieces.reshape(capacity, ep_count, model_width),
        "ep",
        split_axis=1,
        concat_axis=1,
        tiled=True,
    )
    picked = returned.reshape(-1, model_width)[targets].astype(jnp.float32)
    combined = jnp.sum(
        (picked * weights_flat[:, None]).reshape(group_rows, top_count, model_width), axis=1
    )
    moe_out = lax.psum_scatter(combined.astype(jnp.bfloat16), "tp", scatter_dimension=0, tiled=True)
    return (conv_out, moe_out)


def solution(mesh):
    placed = (
        P("ep", "tp"),
        P(None, "tp"),
        P("tp"),
        P("tp"),
        P("tp", None),
        P(("ep", "tp"), None),
        P(),
        P("ep", None),
        P("ep", None),
        P("ep", None, "tp"),
        P("ep", None, "tp"),
        P("ep", "tp", None),
    )
    return jax.shard_map(
        local,
        mesh=mesh,
        in_specs=placed,
        out_specs=(P(("ep", "tp"), None), P(("ep", "tp"), None)),
        check_vma=False,
    )
```

profile of v0, /device:TPU:0, one launch (start us, length us, event | category | flops | bytes accessed | tf_op | source)
XLA Modules:
  0.0 288.2 jit_solution(171710955497054303)
XLA Ops:
  7.2 0.0 copy-start
  7.2 0.0 all-gather.3.cloned.1.call-start
  7.2 1.2 fusion.50
  8.5 1.8 fusion.52
  10.3 0.0 all-gather.3.cloned.1.call-update
  10.3 0.0 all-gather.5.cloned.1.call-start
  10.4 0.8 copy.19
  11.2 0.1 eq.29
  11.3 0.1 eq.25
  11.5 0.1 reshape.90
  11.6 1.1 reduce-window.6
  12.8 0.2 slice_reduce_fusion
  13.0 0.1 fusion.54
  13.1 2.4 scatter_custom_fusion
  15.6 14.3 %all-gather.3.cloned.1.call-done = bf16[256,2048]{1,0:T(8,128)(2,1)} async-done(((bf16[64,2048]{1,0:T(8,128)(2,1)}), bf16[256,2048]{1,0:T(8,128)(2,1)}) %all-gather.3.cloned.1.call-update) | async-done | bytes 1048592 | tf_op jit(solution)/shard_map/all_gather | solution.py:55
  29.9 1.3 concatenate.7
  31.2 6.0 %gather_fusion = bf16[1024,2048]{1,0:T(8,128)(2,1)} fusion(bf16[257,2048]{1,0:T(8,128)(2,1)S(1)} %concatenate.7, s32[1024]{0:T(1024)S(1)} %fusion.56), kind=kCustom, calls=%fused_computation | custom fusion | bytes 8392704 | tf_op jit(solution)/shard_map/gather | solution.py:68
  37.2 1.3 constant_dynamic-slice_fusion
  38.5 0.6 copy.27
  39.1 31.4 %all_to_all.10 = bf16[32,8,2048]{2,0,1:T(8,128)(2,1)S(1)} all-to-all(bf16[32,8,2048]{2,0,1:T(8,128)(2,1)S(1)} %copy.27), channel_id=1, replica_groups=mesh['ep'=8,'tp'=4] {'ep'}, dimensions={1} | all-to-all | bytes 2097152 | tf_op jit(solution)/shard_map/all_to_all | solution.py:71
  70.5 0.0 copy-start.1
  70.5 0.0 copy-start.2
  70.5 1.6 copy.23
  72.1 0.0 copy-start.4
  72.1 0.0 copy-start.5
  72.1 0.0 all-gather.5.cloned.1.call-update
  72.1 0.0 reduce-scatter.3.cloned.1.call-start
  72.2 0.0 copy-done.1
  72.2 3.4 %collective-permute-start = (bf16[30,512]{1,0:T(8,128)(2,1)S(1)}, bf16[30,512]{1,0:T(8,128)(2,1)S(1)}, u32[]{:S(2)}, u32[]{:S(2)}) collective-permute-start(bf16[30,512]{1,0:T(8,128)(2,1)S(1)} %slice.192), channel_id=1, source_target_pairs={{0,4},{4,8},{8,12},{12,16},{16,20},{20,24},{24,28},{1,5},{5,9},{9,... | collective-permute-start | bytes 92168 | tf_op jit(solution)/shard_map/ppermute | solution.py:10
  75.6 0.0 copy-done.2
  75.6 1.5 collective-permute-done
  77.1 11.2 %fusion.64 = (f32[1024]{0:T(1024)S(1)}, f32[1024]{0:T(1024)S(1)}, f32[1024,512]{1,0:T(8,128)}) fusion(f32[512]{0:T(512)S(1)} %bitcast.105, bf16[1024,512]{1,0:T(8,128)(2,1)S(1)} %copy-done.1, f32[512]{0:T(512)S(1)} %bitcast.104, bf16[30,512]{1,0:T(8,128)(2,1)S(1)} %collective-permute-done, f32[512]{0:T(512)S(1)} %bitcast.103, f32[512]{0:T(512)S(1)} %bitcast.102, ...), kind=kLoop, calls=%fused_computation.119 | loop fusion | flops 96991232 | bytes 3248128 | tf_op jit(solution)/shard_map/reduce_sum | solution.py:38
  88.3 7.0 %all-reduce.1 = (f32[1024]{0:T(1024)S(1)}, f32[1024]{0:T(1024)S(1)}) all-reduce(f32[1024]{0:T(1024)S(1)} %get-tuple-element.3, f32[1024]{0:T(1024)S(1)} %get-tuple-element.2), channel_id=1, replica_groups=mesh['ep'=8,'tp'=4] {'tp'}, use_global_device_ids=true, to_apply=%region_3.0 | all-reduce | flops 2048 | bytes 16384 | tf_op jit(solution)/shard_map/psum | solution.py:38
  95.3 0.0 copy-done
  95.3 0.0 copy-done.4
  95.3 0.0 copy-done.5
  95.3 6.3 %convolution_convert_fusion = bf16[1024,2048]{1,0:T(8,128)(2,1)} fusion(bf16[512,2048]{1,0:T(8,128)(2,1)S(1)} %copy-done, f32[1024,512]{1,0:T(8,128)} %get-tuple-element.6, f32[512]{0:T(512)S(1)} %copy-done.4, f32[512]{0:T(512)S(1)} %copy-done.5, f32[1024]{0:T(1024)S(1)} %get-tuple-element.39, f32[1024]{0:T(1024)S(1)} %get-tuple-element.38), kind=kOutput, calls=%fused_computation.39 | convolution fusion | flops 2154299392 | bytes 8400896 | tf_op jit(solution)/shard_map/dot_general | solution.py:44
  101.6 0.0 reduce-scatter.3.cloned.1.call-update
  101.6 3.5 %all-gather.5.cloned.1.call-done = bf16[128,8,2048]{2,1,0:T(8,128)(2,1)} async-done(((bf16[32,8,2048]{2,1,0:T(8,128)(2,1)}), bf16[128,8,2048]{2,1,0:T(8,128)(2,1)}) %all-gather.5.cloned.1.call-update) | async-done | bytes 4194320 | tf_op jit(solution)/shard_map/all_gather | solution.py:72
  105.1 6.6 %fusion.2 = f32[1024,512]{1,0:T(8,128)} fusion(bf16[128,8,2048]{2,1,0:T(8,128)(2,1)} %all-gather.5.cloned.1.call-done, bf16[1,2048,512]{2,1,0:T(8,128)(2,1)} %param.21), kind=kOutput, calls=%fused_computation.34 | convolution fusion | flops 2147483648 | bytes 8388608 | tf_op jit(solution)/shard_map/dot_general | solution.py:74
  111.7 11.5 %convert_bitcast_fusion = bf16[128,8,2048]{2,1,0:T(8,128)(2,1)} fusion(bf16[1,512,2048]{2,1,0:T(8,128)(2,1)} %param.23, f32[1024,512]{1,0:T(8,128)} %fusion.2, bf16[1,2048,512]{2,1,0:T(8,128)(2,1)} %param.22, bf16[128,8,2048]{2,1,0:T(8,128)(2,1)} %all-gather.5.cloned.1.call-done), kind=kOutput, calls=%fused_computation.38 | convolution fusion | flops 4300210176 | bytes 14680064 | tf_op jit(solution)/shard_map/dot_general | solution.py:79
  123.2 6.4 %copy.24 = bf16[128,8,2048]{2,0,1:T(8,128)(2,1)} copy(bf16[128,8,2048]{2,1,0:T(8,128)(2,1)} %convert_bitcast_fusion) | data formatting | bytes 8388608 | tf_op jit(solution)/shard_map/reshape | solution.py:81
  129.6 0.0 copy-start.3
  129.6 5.4 %all-to-all-start.1 = ((bf16[128,8,2048]{2,0,1:T(8,128)(2,1)}), bf16[128,8,2048]{2,0,1:T(8,128)(2,1)}, u32[]{:S(2)}, u32[]{:S(2)}) async-start(bf16[128,8,2048]{2,0,1:T(8,128)(2,1)} %copy.24), calls=%async_computation.2 | async-start | bytes 8388608 | tf_op jit(solution)/shard_map/all_to_all | solution.py:80
  135.1 0.3 reduce-scatter.5.cloned.1.call-start
  135.3 0.0 copy-done.3
  135.3 0.1 copy.26
  135.5 93.3 %all-to-all-done.1 = bf16[128,8,2048]{2,0,1:T(8,128)(2,1)} async-done(((bf16[128,8,2048]{2,0,1:T(8,128)(2,1)}), bf16[128,8,2048]{2,0,1:T(8,128)(2,1)}, u32[]{:S(2)}, u32[]{:S(2)}) %all-to-all-start.1) | async-done | bytes 4194336 | tf_op jit(solution)/shard_map/all_to_all | solution.py:80
  228.8 6.5 %copy.29 = bf16[128,8,2048]{2,1,0:T(8,128)(2,1)} copy(bf16[128,8,2048]{2,0,1:T(8,128)(2,1)} %all-to-all-done.1) | data formatting | bytes 8388608 | tf_op jit(solution)/shard_map/all_to_all | solution.py:80
  235.2 8.0 %gather_fusion.1 = bf16[512,2048]{1,0:T(8,128)(2,1)} fusion(bf16[1024,2048]{1,0:T(8,128)(2,1)} %bitcast.70, s32[1024]{0:T(1024)S(1)} %pad_clamp_fusion), kind=kCustom, calls=%fused_computation.1 | custom fusion | bytes 4196352 | tf_op jit(solution)/shard_map/gather | solution.py:87
  243.2 5.4 %reshape.95 = f32[256,2,2048]{2,1,0:T(2,128)} reshape(bf16[512,2048]{1,0:T(8,128)(2,1)} %gather_fusion.1) | data formatting | bytes 6291456 | tf_op jit(solution)/shard_map/convert_element_type | solution.py:87
  248.6 10.0 %multiply_reduce_fusion = bf16[256,2048]{1,0:T(8,128)(2,1)} fusion(f32[256,2,2048]{2,1,0:T(2,128)} %reshape.95, f32[256,2]{1,0:T(8,128)S(1)} %copy.26), kind=kLoop, calls=%fused_computation.37 | loop fusion | flops 1572864 | bytes 5244928 | tf_op jit(solution)/shard_map/reduce_sum | solution.py:88
  258.6 0.0 reduce-scatter.5.cloned.1.call-update
  258.6 0.0 reduce-scatter.3.cloned.1.call-done
  258.6 23.0 %reduce-scatter.5.cloned.1.call-done = bf16[64,2048]{1,0:T(8,128)(2,1)} async-done(((bf16[256,2048]{1,0:T(8,128)(2,1)}), bf16[64,2048]{1,0:T(8,128)(2,1)}) %reduce-scatter.5.cloned.1.call-update) | async-done | bytes 262160 | tf_op jit(solution)/shard_map/reduce_scatter | solution.py:91
  (13 shorter events, 0.2 us)
Async XLA Ops:
  7.2 88.1 %copy-start = (bf16[512,2048]{1,0:T(8,128)(2,1)S(1)}, bf16[512,2048]{1,0:T(8,128)(2,1)}, u32[]{:S(2)}) copy-start(bf16[512,2048]{1,0:T(8,128)(2,1)} %param.16) | copy-start | bytes 6291460
  7.2 22.7 %all-gather.3.cloned.1.call-start = ((), (), s32[]{:S(2)}) async-start(), calls=%async_computation.5 | async-start | bytes 1310720 | tf_op jit(solution)/shard_map/all_gather | solution.py:55
  10.3 94.8 %all-gather.5.cloned.1.call-start = ((), (), s32[]{:S(2)}) async-start(), calls=%async_computation.6 | async-start | bytes 5242880 | tf_op jit(solution)/shard_map/all_gather | solution.py:72
  70.5 1.6 copy-start.1
  70.5 5.0 %copy-start.2 = (bf16[31,512]{1,0:T(8,128)(2,1)S(1)}, bf16[31,512]{1,0:T(8,128)(2,1)}, u32[]{:S(2)}) copy-start(bf16[31,512]{1,0:T(8,128)(2,1)} %param.13) | copy-start | bytes 95236
  72.1 23.2 %copy-start.4 = (f32[512]{0:T(512)S(1)}, f32[512]{0:T(512)}, u32[]{:S(2)}) copy-start(f32[512]{0:T(512)} %param.15) | copy-start | bytes 6148
  72.1 23.2 %copy-start.5 = (f32[512]{0:T(512)S(1)}, f32[512]{0:T(512)}, u32[]{:S(2)}) copy-start(f32[512]{0:T(512)} %param.14) | copy-start | bytes 6148
  72.1 186.5 %reduce-scatter.3.cloned.1.call-start = ((), (), s32[]{:S(2)}) async-start(), calls=%async_computation.4 | async-start | bytes 5242880 | tf_op jit(solution)/shard_map/reduce_scatter | solution.py:43
  72.2 5.0 %collective-permute-start = (bf16[30,512]{1,0:T(8,128)(2,1)S(1)}, bf16[30,512]{1,0:T(8,128)(2,1)S(1)}, u32[]{:S(2)}, u32[]{:S(2)}) collective-permute-start(bf16[30,512]{1,0:T(8,128)(2,1)S(1)} %slice.192), channel_id=1, source_target_pairs={{0,4},{4,8},{8,12},{12,16},{16,20},{20,24},{24,28},{1,5},{5,9},{9,... | collective-permute-start | bytes 92168 | tf_op jit(solution)/shard_map/ppermute | solution.py:10
  129.6 5.7 %copy-start.3 = (f32[256,2]{0,1:T(2,128)S(1)}, f32[256,2]{0,1:T(2,128)}, u32[]{:S(2)}) copy-start(f32[256,2]{0,1:T(2,128)} %param.20) | copy-start | bytes 6148
  129.6 99.1 %all-to-all-start.1 = ((bf16[128,8,2048]{2,0,1:T(8,128)(2,1)}), bf16[128,8,2048]{2,0,1:T(8,128)(2,1)}, u32[]{:S(2)}, u32[]{:S(2)}) async-start(bf16[128,8,2048]{2,0,1:T(8,128)(2,1)} %copy.24), calls=%async_computation.2 | async-start | bytes 8388608 | tf_op jit(solution)/shard_map/all_to_all | solution.py:80
  135.1 146.6 %reduce-scatter.5.cloned.1.call-start = ((), (), s32[]{:S(2)}) async-start(), calls=%async_computation.7 | async-start | bytes 1310720 | tf_op jit(solution)/shard_map/reduce_scatter | solution.py:91
Sparse Core Ops, SparseCore 0:
  10.4 19.4 all-gather.2
  72.2 32.8 all-gather.4
  108.2 44.5 reduce-scatter.2
  258.7 22.9 reduce-scatter.4
where the time goes:
time: 289 us; the launch traced here: 288 us
  waiting for transfers between devices  136 us (47%)
  local copies, waits for them, and re-layouts  41.2 us (14%)
  blocking collectives  38.4 us (13%)
  other arithmetic  25.5 us (9%)
  matrix products  24.4 us (8%)
  between operations  14 us (5%)
  starting transfers between devices  9.18 us (3%)
    all_to_all x1, waiting for transfers between devices, local(): lax.all_to_all(pieces.reshape(capacity, ep_count, model_width), 'ep', spl...  93.3 us
    all_to_all x1, blocking collectives, local(): lax.all_to_all(own_slots, 'ep', split_axis=1, concat_axis=1, tiled=True)  31.4 us
    reduce_scatter x1, waiting for transfers between devices, local(): lax.psum_scatter(combined.astype(jnp.bfloat16), 'tp', scatter_dimension=0...  23 us
    all_gather x1, waiting for transfers between devices, local(): group = lax.all_gather(normed, 'tp', axis=0, tiled=True)  14.3 us
    dot_general x1, matrix products, local(): jnp.dot(hidden, down_proj[0], preferred_element_type=jnp.float32)  11.5 us
    reduce_sum x1, other arithmetic, local(): jnp.sum(mixed, axis=1)  11.2 us
    reduce_sum x1, other arithmetic, local(): jnp.sum((picked * weights_flat[:, None]).reshape(group_rows, top_count, m...  9.96 us
    gather x1, local copies, waits for them, and re-layouts, local(): picked = returned.reshape(-1, model_width)[targets].astype(jnp.float32)  7.95 us
  transfers between devices with their start and end apart: 6, of which 5 were waited for; matrix products, arithmetic and copies ran while one was open for 27% of the time, Pallas kernels for 0%

commit v1 on v0

--- a/solution.py
+++ b/solution.py
@@ -77,12 +77,18 @@
     )
     weights_flat = route_weights.reshape(-1)
     pieces = jnp.dot(hidden, down_proj[0], preferred_element_type=jnp.float32).astype(jnp.bfloat16)
-    returned = lax.all_to_all(
-        pieces.reshape(capacity, ep_count, model_width),
-        "ep",
-        split_axis=1,
-        concat_axis=1,
-        tiled=True,
+    returned = jnp.concatenate(
+        lax.all_to_all(
+            jnp.stack(
+                jnp.split(
+                    pieces.reshape(capacity, ep_count, model_width), lax.axis_size("ep"), axis=1
+                )
+            ),
+            "ep",
+            0,
+            0,
+        ),
+        axis=1,
     )
     picked = returned.reshape(-1, model_width)[targets].astype(jnp.float32)
     combined = jnp.sum(

time: 289 us -> 314 us (1.087)
  local copies, waits for them, and re-layouts: 41.2 us -> 66.7 us
    split x0 -> x1, local copies, waits for them, and re-layouts: none -> 22.6 us  [local(): jnp.split(pieces.reshape(capacity, ep_count, model_width), lax.axis_size(...]
    unnamed x15 -> x26, local copies, waits for them, and re-layouts: 1.55 us -> 9.39 us
    all_to_all x1 -> x0, local copies, waits for them, and re-layouts: 6.46 us -> none  [local(): lax.all_to_all(pieces.reshape(capacity, ep_count, model_width), 'ep', spl...]
  transfers between devices with their start and end apart: 6 -> 6, of which waited for: 5 -> 5; matrix products, arithmetic and copies ran while one was open for 27% -> 33% of each run, Pallas kernels for 0% -> 0%
where the time goes in v1:
time: 314 us; the launch traced here: 313 us
  waiting for transfers between devices  136 us (43%)
  local copies, waits for them, and re-layouts  66.7 us (21%)
  blocking collectives  38.4 us (12%)
  other arithmetic  25.5 us (8%)
  matrix products  23.5 us (7%)
  between operations  14 us (4%)
  starting transfers between devices  9.18 us (3%)
    all_to_all x1, waiting for transfers between devices, local(): lax.all_to_all(jnp.stack(jnp.split(pieces.reshape(capacity, ep_count, mod...  93.5 us
    all_to_all x1, blocking collectives, local(): lax.all_to_all(own_slots, 'ep', split_axis=1, concat_axis=1, tiled=True)  31.4 us
    reduce_scatter x1, waiting for transfers between devices, local(): lax.psum_scatter(combined.astype(jnp.bfloat16), 'tp', scatter_dimension=0...  23 us
    split x1, local copies, waits for them, and re-layouts, local(): jnp.split(pieces.reshape(capacity, ep_count, model_width), lax.axis_size(...  22.6 us
    all_gather x1, waiting for transfers between devices, local(): group = lax.all_gather(normed, 'tp', axis=0, tiled=True)  14.3 us
    dot_general x1, matrix products, local(): jnp.dot(hidden, down_proj[0], preferred_element_type=jnp.float32)  11.3 us
    reduce_sum x1, other arithmetic, local(): jnp.sum(mixed, axis=1)  11.2 us
    reduce_sum x1, other arithmetic, local(): jnp.sum((picked * weights_flat[:, None]).reshape(group_rows, top_count, m...  9.96 us
  transfers between devices with their start and end apart: 6, of which 5 were waited for; matrix products, arithmetic and copies ran while one was open for 33% of the time, Pallas kernels for 0%

profile of v1, /device:TPU:0, one launch (start us, length us, event | category | flops | bytes accessed | tf_op | source)
XLA Modules:
  0.0 313.1 jit_solution(10703415528408597307)
XLA Ops:
  7.2 0.0 copy-start
  7.2 0.0 all-gather.3.cloned.1.call-start
  7.2 1.2 fusion.50
  8.5 1.8 fusion.52
  10.3 0.0 all-gather.3.cloned.1.call-update
  10.3 0.0 all-gather.5.cloned.1.call-start
  10.4 0.8 copy.36
  11.2 0.1 eq.29
  11.3 0.1 eq.25
  11.5 0.1 reshape.90
  11.6 1.1 reduce-window.6
  12.8 0.2 slice_reduce_fusion
  13.0 0.1 fusion.62
  13.1 2.4 scatter_custom_fusion
  15.6 14.3 %all-gather.3.cloned.1.call-done = bf16[256,2048]{1,0:T(8,128)(2,1)} async-done(((bf16[64,2048]{1,0:T(8,128)(2,1)}), bf16[256,2048]{1,0:T(8,128)(2,1)}) %all-gather.3.cloned.1.call-update) | async-done | bytes 1048592 | tf_op jit(solution)/shard_map/all_gather | solution.py:55
  29.9 1.3 concatenate.7
  31.2 6.0 %gather_fusion = bf16[1024,2048]{1,0:T(8,128)(2,1)} fusion(bf16[257,2048]{1,0:T(8,128)(2,1)S(1)} %concatenate.7, s32[1024]{0:T(1024)S(1)} %fusion.64), kind=kCustom, calls=%fused_computation | custom fusion | bytes 8392704 | tf_op jit(solution)/shard_map/gather | solution.py:68
  37.2 1.3 constant_dynamic-slice_fusion
  38.5 0.6 copy.51
  39.1 31.4 %all_to_all.10 = bf16[32,8,2048]{2,0,1:T(8,128)(2,1)S(1)} all-to-all(bf16[32,8,2048]{2,0,1:T(8,128)(2,1)S(1)} %copy.51), channel_id=1, replica_groups=mesh['ep'=8,'tp'=4] {'ep'}, dimensions={1} | all-to-all | bytes 2097152 | tf_op jit(solution)/shard_map/all_to_all | solution.py:71
  70.5 0.0 copy-start.2
  70.5 0.0 copy-start.3
  70.5 1.6 copy.40
  72.1 0.0 copy-start.6
  72.1 0.0 copy-start.7
  72.1 0.0 all-gather.5.cloned.1.call-update
  72.1 0.0 reduce-scatter.3.cloned.1.call-start
  72.2 0.0 copy-done.2
  72.2 3.4 %collective-permute-start = (bf16[30,512]{1,0:T(8,128)(2,1)S(1)}, bf16[30,512]{1,0:T(8,128)(2,1)S(1)}, u32[]{:S(2)}, u32[]{:S(2)}) collective-permute-start(bf16[30,512]{1,0:T(8,128)(2,1)S(1)} %slice.192), channel_id=1, source_target_pairs={{0,4},{4,8},{8,12},{12,16},{16,20},{20,24},{24,28},{1,5},{5,9},{9,... | collective-permute-start | bytes 92168 | tf_op jit(solution)/shard_map/ppermute | solution.py:10
  75.6 0.0 copy-done.3
  75.6 1.5 collective-permute-done
  77.1 11.2 %fusion.72 = (f32[1024]{0:T(1024)S(1)}, f32[1024]{0:T(1024)S(1)}, f32[1024,512]{1,0:T(8,128)}) fusion(f32[512]{0:T(512)S(1)} %bitcast.138, bf16[1024,512]{1,0:T(8,128)(2,1)S(1)} %copy-done.2, f32[512]{0:T(512)S(1)} %bitcast.137, bf16[30,512]{1,0:T(8,128)(2,1)S(1)} %collective-permute-done, f32[512]{0:T(512)S(1)} %bitcast.136, f32[512]{0:T(512)S(1)} %bitcast.135, ...), kind=kLoop, calls=%fused_computation.135 | loop fusion | flops 96991232 | bytes 3248128 | tf_op jit(solution)/shard_map/reduce_sum | solution.py:38
  88.3 7.0 %all-reduce.1 = (f32[1024]{0:T(1024)S(1)}, f32[1024]{0:T(1024)S(1)}) all-reduce(f32[1024]{0:T(1024)S(1)} %get-tuple-element.3, f32[1024]{0:T(1024)S(1)} %get-tuple-element.2), channel_id=1, replica_groups=mesh['ep'=8,'tp'=4] {'tp'}, use_global_device_ids=true, to_apply=%region_3.0 | all-reduce | flops 2048 | bytes 16384 | tf_op jit(solution)/shard_map/psum | solution.py:38
  95.3 0.0 copy-done
  95.3 0.0 copy-done.6
  95.3 0.0 copy-done.7
  95.3 6.3 %convolution_convert_fusion = bf16[1024,2048]{1,0:T(8,128)(2,1)} fusion(bf16[512,2048]{1,0:T(8,128)(2,1)S(1)} %copy-done, f32[1024,512]{1,0:T(8,128)} %get-tuple-element.6, f32[512]{0:T(512)S(1)} %copy-done.6, f32[512]{0:T(512)S(1)} %copy-done.7, f32[1024]{0:T(1024)S(1)} %get-tuple-element.47, f32[1024]{0:T(1024)S(1)} %get-tuple-element.46), kind=kOutput, calls=%fused_computation.39 | convolution fusion | flops 2154299392 | bytes 8400896 | tf_op jit(solution)/shard_map/dot_general | solution.py:44
  101.6 0.0 reduce-scatter.3.cloned.1.call-update
  101.6 3.5 %all-gather.5.cloned.1.call-done = bf16[128,8,2048]{2,1,0:T(8,128)(2,1)} async-done(((bf16[32,8,2048]{2,1,0:T(8,128)(2,1)}), bf16[128,8,2048]{2,1,0:T(8,128)(2,1)}) %all-gather.5.cloned.1.call-update) | async-done | bytes 4194320 | tf_op jit(solution)/shard_map/all_gather | solution.py:72
  105.1 0.0 copy-done.5
  105.1 5.9 %fusion.2 = f32[1024,512]{1,0:T(8,128)} fusion(bf16[128,8,2048]{2,1,0:T(8,128)(2,1)} %all-gather.5.cloned.1.call-done, bf16[1,2048,512]{2,1,0:T(8,128)(2,1)S(1)} %copy-done.5), kind=kOutput, calls=%fused_computation.34 | convolution fusion | flops 2147483648 | bytes 8388608 | tf_op jit(solution)/shard_map/dot_general | solution.py:74
  111.0 11.3 %convert_bitcast_fusion = bf16[128,8,2048]{2,1,0:T(8,128)(2,1)} fusion(bf16[1,512,2048]{2,1,0:T(8,128)(2,1)} %param.23, f32[1024,512]{1,0:T(8,128)} %fusion.2, bf16[1,2048,512]{2,1,0:T(8,128)(2,1)} %param.22, bf16[128,8,2048]{2,1,0:T(8,128)(2,1)} %all-gather.5.cloned.1.call-done), kind=kOutput, calls=%fused_computation.38 | convolution fusion | flops 4300210176 | bytes 14680064 | tf_op jit(solution)/shard_map/dot_general | solution.py:79
  122.3 22.6 %fusion.73 = (bf16[128,1,2048]{2,1,0:T(2,128)(2,1)S(1)}, bf16[128,1,2048]{2,1,0:T(2,128)(2,1)S(1)}, bf16[128,1,2048]{2,1,0:T(2,128)(2,1)S(1)}, bf16[128,1,2048]{...) fusion(bf16[128,8,2048]{2,1,0:T(8,128)(2,1)} %convert_bitcast_f, ...), kind=kLoop, calls=%fused_computation.136 | loop fusion | bytes 8388608 | tf_op jit(solution)/shard_map/split | solution.py:83
  144.9 1.1 fusion.60
  146.1 1.2 fusion.59
  147.3 1.1 fusion.58
  148.4 1.1 fusion.57
  149.5 1.1 fusion.56
  150.6 1.1 fusion.55
  151.7 1.1 fusion.54
  152.8 1.1 fusion.53
  153.9 5.7 %all-to-all-start.1 = ((bf16[8,128,1,2048]{3,1,2,0:T(8,128)(2,1)}), bf16[8,128,1,2048]{3,1,2,0:T(8,128)(2,1)}, u32[]{:S(2)}, u32[]{:S(2)}) async-start(bf16[8,128,1,2048]{3,1,2,0:T(8,128)(2,1)} %fusion.53), calls=%async_computation.2 | async-start | bytes 8388608 | tf_op jit(solution)/shard_map/all_to_all | solution.py:81
  159.5 0.0 reduce-scatter.5.cloned.1.call-start
  159.6 0.0 copy-done.4
  159.6 0.1 copy.50
  159.8 93.5 %all-to-all-done.1 = bf16[8,128,1,2048]{3,1,2,0:T(8,128)(2,1)} async-done(((bf16[8,128,1,2048]{3,1,2,0:T(8,128)(2,1)}), bf16[8,128,1,2048]{3,1,2,0:T(8,128)(2,1)}, u32[]{:S(2)}, u32[]{:S(2)}) %all-to-all-start.1) | async-done | bytes 4194336 | tf_op jit(solution)/shard_map/all_to_all | solution.py:81
  253.2 6.5 %copy.85 = bf16[128,8,1,2048]{3,1,0,2:T(8,128)(2,1)} copy(bf16[128,8,1,2048]{3,0,2,1:T(8,128)(2,1)} %bitcast.49) | data formatting | bytes 8388608 | tf_op jit(solution)/shard_map/reshape | solution.py:80
  259.7 8.2 %gather_fusion.1 = bf16[512,2048]{1,0:T(8,128)(2,1)} fusion(bf16[1024,2048]{1,0:T(8,128)(2,1)} %bitcast.103, s32[1024]{0:T(1024)S(1)} %pad_clamp_fusion), kind=kCustom, calls=%fused_computation.1 | custom fusion | bytes 4196352 | tf_op jit(solution)/shard_map/gather | solution.py:93
  267.9 5.6 %reshape.95 = f32[256,2,2048]{2,1,0:T(2,128)} reshape(bf16[512,2048]{1,0:T(8,128)(2,1)} %gather_fusion.1) | data formatting | bytes 6291456 | tf_op jit(solution)/shard_map/convert_element_type | solution.py:93
  273.5 10.0 %multiply_reduce_fusion = bf16[256,2048]{1,0:T(8,128)(2,1)} fusion(f32[256,2,2048]{2,1,0:T(2,128)} %reshape.95, f32[256,2]{1,0:T(8,128)S(1)} %copy.50), kind=kLoop, calls=%fused_computation.37 | loop fusion | flops 1572864 | bytes 5244928 | tf_op jit(solution)/shard_map/reduce_sum | solution.py:94
  283.4 0.0 reduce-scatter.5.cloned.1.call-update
  283.5 0.0 reduce-scatter.3.cloned.1.call-done
  283.5 23.0 %reduce-scatter.5.cloned.1.call-done = bf16[64,2048]{1,0:T(8,128)(2,1)} async-done(((bf16[256,2048]{1,0:T(8,128)(2,1)}), bf16[64,2048]{1,0:T(8,128)(2,1)}) %reduce-scatter.5.cloned.1.call-update) | async-done | bytes 262160 | tf_op jit(solution)/shard_map/reduce_scatter | solution.py:97
  306.5 0.0 copy-done.1
  (16 shorter events, 0.2 us)
Async XLA Ops:
  7.2 88.1 %copy-start = (bf16[512,2048]{1,0:T(8,128)(2,1)S(1)}, bf16[512,2048]{1,0:T(8,128)(2,1)}, u32[]{:S(2)}) copy-start(bf16[512,2048]{1,0:T(8,128)(2,1)} %param.16) | copy-start | bytes 6291460
  7.2 22.7 %all-gather.3.cloned.1.call-start = ((), (), s32[]{:S(2)}) async-start(), calls=%async_computation.5 | async-start | bytes 1310720 | tf_op jit(solution)/shard_map/all_gather | solution.py:55
  10.3 94.8 %all-gather.5.cloned.1.call-start = ((), (), s32[]{:S(2)}) async-start(), calls=%async_computation.6 | async-start | bytes 5242880 | tf_op jit(solution)/shard_map/all_gather | solution.py:72
  70.5 1.6 copy-start.2
  70.5 5.0 %copy-start.3 = (bf16[31,512]{1,0:T(8,128)(2,1)S(1)}, bf16[31,512]{1,0:T(8,128)(2,1)}, u32[]{:S(2)}) copy-start(bf16[31,512]{1,0:T(8,128)(2,1)} %param.13) | copy-start | bytes 95236
  72.1 23.2 %copy-start.6 = (f32[512]{0:T(512)S(1)}, f32[512]{0:T(512)}, u32[]{:S(2)}) copy-start(f32[512]{0:T(512)} %param.15) | copy-start | bytes 6148
  72.1 23.2 %copy-start.7 = (f32[512]{0:T(512)S(1)}, f32[512]{0:T(512)}, u32[]{:S(2)}) copy-start(f32[512]{0:T(512)} %param.14) | copy-start | bytes 6148
  72.1 211.4 %reduce-scatter.3.cloned.1.call-start = ((), (), s32[]{:S(2)}) async-start(), calls=%async_computation.4 | async-start | bytes 5242880 | tf_op jit(solution)/shard_map/reduce_scatter | solution.py:43
  72.2 5.0 %collective-permute-start = (bf16[30,512]{1,0:T(8,128)(2,1)S(1)}, bf16[30,512]{1,0:T(8,128)(2,1)S(1)}, u32[]{:S(2)}, u32[]{:S(2)}) collective-permute-start(bf16[30,512]{1,0:T(8,128)(2,1)S(1)} %slice.192), channel_id=1, source_target_pairs={{0,4},{4,8},{8,12},{12,16},{16,20},{20,24},{24,28},{1,5},{5,9},{9,... | collective-permute-start | bytes 92168 | tf_op jit(solution)/shard_map/ppermute | solution.py:10
  101.6 3.5 %copy-start.5 = (bf16[1,2048,512]{2,1,0:T(8,128)(2,1)S(1)}, bf16[1,2048,512]{2,1,0:T(8,128)(2,1)}, u32[]{:S(2)}) copy-start(bf16[1,2048,512]{2,1,0:T(8,128)(2,1)} %param.21) | copy-start | bytes 6291460
  153.9 5.7 %copy-start.4 = (f32[256,2]{0,1:T(2,128)S(1)}, f32[256,2]{0,1:T(2,128)}, u32[]{:S(2)}) copy-start(f32[256,2]{0,1:T(2,128)} %param.20) | copy-start | bytes 6148
  153.9 99.3 %all-to-all-start.1 = ((bf16[8,128,1,2048]{3,1,2,0:T(8,128)(2,1)}), bf16[8,128,1,2048]{3,1,2,0:T(8,128)(2,1)}, u32[]{:S(2)}, u32[]{:S(2)}) async-start(bf16[8,128,1,2048]{3,1,2,0:T(8,128)(2,1)} %fusion.53), calls=%async_computation.2 | async-start | bytes 8388608 | tf_op jit(solution)/shard_map/all_to_all | solution.py:81
  159.5 147.0 %reduce-scatter.5.cloned.1.call-start = ((), (), s32[]{:S(2)}) async-start(), calls=%async_computation.7 | async-start | bytes 1310720 | tf_op jit(solution)/shard_map/reduce_scatter | solution.py:97
  267.9 38.6 %copy-start.1 = (bf16[512,2048]{1,0:T(8,128)(2,1)S(1)}, bf16[512,2048]{1,0:T(8,128)(2,1)}, u32[]{:S(2)}) copy-start(bf16[512,2048]{1,0:T(8,128)(2,1)} %param.16) | copy-start | bytes 6291460
Sparse Core Ops, SparseCore 0:
  10.4 19.4 all-gather.2
  72.2 32.8 all-gather.4
  108.2 44.5 reduce-scatter.2
  283.6 22.9 reduce-scatter.4
